TPU v7x, 1024 devices: a whole 4x8x16 slice. The times are simulated.
1024 devices in a mesh: fs: 32 (over z, core), tp: 32 (over y, x).
Axes of the slice: x: 4, y: 8, z: 16, core: 2. Of those that a mesh axis runs over, the one named last changes fastest.
Arguments:
- latent: bfloat16 [65536, 1024], P('fs'), may hold values from -6 to 6
- key_cotangent: bfloat16 [65536, 4096], P('fs', 'tp'), may hold values from -0.0234375 to 0.0234375
- value_cotangent: bfloat16 [65536, 4096], P('fs', 'tp'), may hold values from -0.0234375 to 0.0234375
- key_weight: float32 [1024, 4096], P('fs', 'tp'), may hold values from -50 to 50
- value_weight: float32 [1024, 4096], P('fs', 'tp'), may hold values from -50 to 50
- key_projector: bfloat16 [1024, 256], replicated, may hold values from -0.1875 to 0.1875
- value_projector: bfloat16 [1024, 256], replicated, may hold values from -0.1875 to 0.1875
- key_first: float32 [256, 4096], P(None, 'tp'), may hold values from -6 to 6
- key_second: float32 [256, 4096], P(None, 'tp'), may hold values from 0.3 to 3
- value_first: float32 [256, 4096], P(None, 'tp'), may hold values from -6 to 6
- value_second: float32 [256, 4096], P(None, 'tp'), may hold values from 0.3 to 3
Outputs:
- key_renewed: float32 [1024, 4096], P('fs', 'tp')
- value_renewed: float32 [1024, 4096], P('fs', 'tp')
- key_step: float32 [1024, 4096], P('fs', 'tp')
- value_step: float32 [1024, 4096], P('fs', 'tp')
- key_first_new: float32 [256, 4096], P(None, 'tp')
- key_second_new: float32 [256, 4096], P(None, 'tp')
- value_first_new: float32 [256, 4096], P(None, 'tp')
- value_second_new: float32 [256, 4096], P(None, 'tp')
- key_copy: bfloat16 [1024, 4096], P(None, 'tp')
- value_copy: bfloat16 [1024, 4096], P(None, 'tp')
All inputs are finite; a program needn't handle non-finite values.
Results may differ from a plain program's by a relative error of at most 0.015.
Values may be sent and summed in bfloat16 or wider, within the bound.
No kernel may reach another device: no remote copies, remote signals or barrier semaphores. Data moves between devices by JAX's collectives and lax.ppermute only.
A program may use at most 32 MiB of HBM per device.

v0:
```python
import functools

import jax
import jax.numpy as jnp
from jax import lax
from jax.sharding import Mesh
from jax.sharding import PartitionSpec as P

FS = ("fs_0", "fs_1")
FS_TP = ("fs_0", "fs_1", "tp_0", "tp_1")
TP = ("tp_0", "tp_1")


EPSILON = 1e-08
FIRST_DECAY = 0.7
SECOND_DECAY = 0.8
LEARN_RATE = 0.2


def over_axes(array, axes):
    return functools.reduce(lax.psum, axes, array)


def total_of_pieces(array, axis):
    pieces = lax.all_gather(array, axis).astype(jnp.float32)
    return pieces.sum(axis=0)


def sent_together(arrays, axis, dim, along):
    both = jnp.concatenate(arrays, axis=along)
    result, at, done = (lax.all_gather(both, axis, axis=dim, tiled=True), 0, [])
    for a in arrays:
        done.append(lax.slice_in_dim(result, at, at + a.shape[along], axis=along))
        at += a.shape[along]
    return tuple(done)


def contract_rows(left, right):
    return jnp.dot(left.T, right, precision=lax.Precision.HIGHEST)


def moments_and_step(
    weight, factor_rows, projected, first_moment, second, total_squares, entry_count
):
    first_new = FIRST_DECAY * first_moment + (1.0 - FIRST_DECAY) * projected
    second_new = SECOND_DECAY * second + (1.0 - SECOND_DECAY) * projected * projected
    normalized = first_new / (jnp.sqrt(second_new) + EPSILON)
    direction = jnp.dot(
        factor_rows.astype(jnp.float32), normalized, precision=lax.Precision.HIGHEST
    )
    step_scale = LEARN_RATE * jnp.sqrt(total_squares / entry_count)
    weight_step = step_scale * direction
    return (weight - weight_step, weight_step, first_new, second_new)


def body(
    latent,
    key_cotangent,
    value_cotangent,
    key_weight,
    value_weight,
    key_projector,
    value_projector,
    key_first,
    key_second,
    value_first,
    value_second,
):
    row_count = key_weight.shape[0]
    row_start = lax.axis_index(FS) * row_count
    key_rows = lax.dynamic_slice_in_dim(key_projector, row_start, row_count, 0)
    value_rows = lax.dynamic_slice_in_dim(value_projector, row_start, row_count, 0)
    key_squares, value_squares = (
        over_axes(jnp.sum(key_weight * key_weight), FS_TP),
        over_axes(jnp.sum(value_weight * value_weight), FS_TP),
    )
    devices = lax.axis_size(FS) * lax.axis_size(TP)
    key_entries = float(key_weight.size * devices)
    value_entries = float(value_weight.size * devices)
    rank = key_projector.shape[1]
    factors = jnp.concatenate([key_projector, value_projector], axis=1)
    reduced = jnp.dot(latent, factors, preferred_element_type=jnp.float32)
    key_term = contract_rows(reduced[:, :rank], key_cotangent.astype(jnp.float32))
    value_term = contract_rows(reduced[:, rank:], value_cotangent.astype(jnp.float32))
    key_projected, value_projected = (
        total_of_pieces(key_term.astype(jnp.bfloat16), FS).astype(jnp.float32),
        total_of_pieces(value_term.astype(jnp.bfloat16), FS).astype(jnp.float32),
    )
    key_renewed, key_step, key_first_new, key_second_new = moments_and_step(
        key_weight, key_rows, key_projected, key_first, key_second, key_squares, key_entries
    )
    value_renewed, value_step, value_first_new, value_second_new = moments_and_step(
        value_weight,
        value_rows,
        value_projected,
        value_first,
        value_second,
        value_squares,
        value_entries,
    )
    key_copy, value_copy = sent_together(
        (key_renewed.astype(jnp.bfloat16), value_renewed.astype(jnp.bfloat16)), FS, 0, 1
    )
    return (
        key_renewed,
        value_renewed,
        key_step,
        value_step,
        key_first_new,
        key_second_new,
        value_first_new,
        value_second_new,
        key_copy,
        value_copy,
    )


def solution(mesh):
    finer = Mesh(mesh.devices.reshape(16, 2, 8, 4), ("fs_0", "fs_1", "tp_0", "tp_1"))
    return jax.shard_map(
        body,
        mesh=finer,
        in_specs=(
            P(FS, None),
            P(FS, TP),
            P(FS, TP),
            P(FS, TP),
            P(FS, TP),
            P(),
            P(),
            P(None, TP),
            P(None, TP),
            P(None, TP),
            P(None, TP),
        ),
        out_specs=(
            P(FS, TP),
            P(FS, TP),
            P(FS, TP),
            P(FS, TP),
            P(None, TP),
            P(None, TP),
            P(None, TP),
            P(None, TP),
            P(None, TP),
            P(None, TP),
        ),
        check_vma=False,
    )
```

profile of v0, /device:TPU:1, one launch (start us, length us, event | category | flops | bytes accessed | tf_op | source)
XLA Modules:
  0.0 218.8 jit_solution(15390986067735608077)
XLA Ops:
  7.2 0.0 copy-start
  7.2 0.0 copy-start.2
  7.2 0.0 all-gather.5.cloned.1.call-start
  7.2 5.0 %convolution_bitcast_fusion = f32[2048,512]{0,1:T(8,128)S(1)} fusion(bf16[2048,1024]{1,0:T(8,128)(2,1)} %param.11, bf16[1024,256]{1,0:T(8,128)(2,1)} %param.17, bf16[1024,256]{1,0:T(8,128)(2,1)} %param.16), kind=kOutput, calls=%fused_computation.2 | convolution fusion | flops 2149580800 | bytes 9437184 | tf_op jit(solution)/shard_map/dot_general | solution.py:82
  12.2 0.0 copy-start.1
  12.2 1.9 copy-done.1
  14.2 0.0 copy-done
  14.2 0.0 copy-start.11
  14.2 0.0 copy-start.12
  14.2 1.7 fusion.4
  15.9 0.0 copy-start.3
  15.9 0.0 copy-start.4
  15.9 0.0 copy-start.5
  15.9 0.0 copy-start.6
  15.9 0.0 all-gather.5.cloned.1.call-update
  15.9 0.0 all-gather.7.cloned.1.call-start
  15.9 0.0 copy-done.2
  16.0 3.4 %fusion.7 = bf16[256,128]{1,0:T(8,128)(2,1)} fusion(bf16[2048,128]{1,0:T(8,128)(2,1)S(1)} %copy-done.2, f32[2048,512]{0,1:T(8,128)} %copy-done.1), kind=kOutput, calls=%fused_computation.8 | convolution fusion | flops 805339136 | bytes 2686976 | tf_op jit(solution)/shard_map/dot_general | solution.py:39
  19.4 0.0 all-gather.7.cloned.1.call-update
  19.4 0.0 copy-done.11
  19.4 0.0 copy-done.12
  19.4 0.6 multiply_reduce_fusion
  20.0 37.8 %all-reduce = (f32[]{:T(128)}, f32[]{:T(128)}) all-reduce(f32[]{:T(128)} %get-tuple-element.31, f32[]{:T(128)} %get-tuple-element.30), channel_id=1, replica_groups=mesh['fs_0'=16,'fs_1'=2,'tp_0'=8,'tp_1'=4] {'fs_0'}, use_global_device_ids=true, to_apply=%region_1.0 | all-reduce | flops 2 | bytes 16 | tf_op jit(solution)/shard_map/psum | solution.py:21
  57.8 10.5 %all-reduce.3 = (f32[]{:T(128)}, f32[]{:T(128)}) all-reduce(f32[]{:T(128)} %get-tuple-element.10, f32[]{:T(128)} %get-tuple-element.11), channel_id=1, replica_groups=mesh['fs_0'=16,'fs_1'=2,'tp_0'=8,'tp_1'=4] {'fs_1'}, use_global_device_ids=true, to_apply=%region_2.0 | all-reduce | flops 2 | bytes 16 | tf_op jit(solution)/shard_map/psum | solution.py:21
  68.2 15.4 %all-reduce.1 = (f32[]{:T(128)}, f32[]{:T(128)}) all-reduce(f32[]{:T(128)} %get-tuple-element.16, f32[]{:T(128)} %get-tuple-element.17), channel_id=1, replica_groups=mesh['fs_0'=16,'fs_1'=2,'tp_0'=8,'tp_1'=4] {'tp_0'}, use_global_device_ids=true, to_apply=%region_3.0 | all-reduce | flops 2 | bytes 16 | tf_op jit(solution)/shard_map/psum | solution.py:21
  83.6 9.6 %all-reduce.2 = (f32[]{:T(128)}, f32[]{:T(128)}) all-reduce(f32[]{:T(128)} %get-tuple-element.12, f32[]{:T(128)} %get-tuple-element.13), channel_id=1, replica_groups=mesh['fs_0'=16,'fs_1'=2,'tp_0'=8,'tp_1'=4] {'tp_1'}, use_global_device_ids=true, to_apply=%region_4.0 | all-reduce | flops 2 | bytes 16 | tf_op jit(solution)/shard_map/psum | solution.py:21
  94.5 5.7 %all-gather.5.cloned.1.call-done = bf16[8192,128]{1,0:T(8,128)(2,1)} async-done(((bf16[256,128]{1,0:T(8,128)(2,1)}), bf16[8192,128]{1,0:T(8,128)(2,1)}) %all-gather.5.cloned.1.call-update) | async-done | bytes 2097168 | tf_op jit(solution)/shard_map/all_gather | solution.py:25
  100.2 1.9 convert_reduce_fusion.1
  102.1 72.9 %all-gather.7.cloned.1.call-done = bf16[8192,128]{1,0:T(8,128)(2,1)} async-done(((bf16[256,128]{1,0:T(8,128)(2,1)}), bf16[8192,128]{1,0:T(8,128)(2,1)}) %all-gather.7.cloned.1.call-update) | async-done | bytes 2097168 | tf_op jit(solution)/shard_map/all_gather | solution.py:25
  175.1 1.9 convert_reduce_fusion
  176.9 0.0 copy-done.3
  177.0 0.0 copy-done.4
  177.0 0.0 copy-done.5
  177.0 0.0 copy-done.6
  177.0 0.1 fusion.13
  177.1 0.0 copy-start.7
  177.1 0.0 copy-start.8
  177.1 0.0 copy-start.9
  177.1 0.0 copy-start.10
  177.1 1.6 fusion.24
  178.7 1.6 fusion.25
  180.3 30.8 %all_gather.19 = bf16[1024,256]{1,0:T(8,128)(2,1)S(1)} all-gather(bf16[32,256]{1,0:T(8,128)(2,1)S(1)} %pad_maximum_fusion), channel_id=1, replica_groups=mesh['fs_0'=16,'fs_1'=2,'tp_0'=8,'tp_1'=4] {'fs_0','fs_1'}, dimensions={0}, use_global_device_ids=true | all-gather | bytes 540672 | tf_op jit(solution)/shard_map/all_gather | solution.py:31
  211.1 0.8 fusion.26
  211.9 0.0 copy-done.7
  211.9 0.0 copy-done.8
  211.9 0.0 copy-done.9
  211.9 0.0 copy-done.10
  (1 shorter events, 0.0 us)
Async XLA Ops:
  7.2 7.0 %copy-start = (bf16[2048,128]{1,0:T(8,128)(2,1)S(1)}, bf16[2048,128]{1,0:T(8,128)(2,1)}, u32[]{:S(2)}) copy-start(bf16[2048,128]{1,0:T(8,128)(2,1)} %param.12) | copy-start | bytes 1572868
  7.2 8.8 %copy-start.2 = (bf16[2048,128]{1,0:T(8,128)(2,1)S(1)}, bf16[2048,128]{1,0:T(8,128)(2,1)}, u32[]{:S(2)}) copy-start(bf16[2048,128]{1,0:T(8,128)(2,1)} %param.13) | copy-start | bytes 1572868
  7.2 93.0 %all-gather.5.cloned.1.call-start = ((), (), s32[]{:S(2)}) async-start(), calls=%async_computation | async-start | bytes 2162688 | tf_op jit(solution)/shard_map/all_gather | solution.py:25
  12.2 1.9 copy-start.1
  14.2 5.2 %copy-start.11 = (f32[32,128]{1,0:T(8,128)S(1)}, f32[32,128]{1,0:T(8,128)}, u32[]{:S(2)}) copy-start(f32[32,128]{1,0:T(8,128)} %param.14) | copy-start | bytes 49156
  14.2 5.2 %copy-start.12 = (f32[32,128]{1,0:T(8,128)S(1)}, f32[32,128]{1,0:T(8,128)}, u32[]{:S(2)}) copy-start(f32[32,128]{1,0:T(8,128)} %param.15) | copy-start | bytes 49156
  15.9 161.1 %copy-start.3 = (f32[256,128]{1,0:T(8,128)S(1)}, f32[256,128]{1,0:T(8,128)}, u32[]{:S(2)}) copy-start(f32[256,128]{1,0:T(8,128)} %param.19) | copy-start | bytes 393220
  15.9 161.1 %copy-start.4 = (f32[256,128]{1,0:T(8,128)S(1)}, f32[256,128]{1,0:T(8,128)}, u32[]{:S(2)}) copy-start(f32[256,128]{1,0:T(8,128)} %param.18) | copy-start | bytes 393220
  15.9 161.1 %copy-start.5 = (f32[256,128]{1,0:T(8,128)S(1)}, f32[256,128]{1,0:T(8,128)}, u32[]{:S(2)}) copy-start(f32[256,128]{1,0:T(8,128)} %param.20) | copy-start | bytes 393220
  15.9 161.1 %copy-start.6 = (f32[256,128]{1,0:T(8,128)S(1)}, f32[256,128]{1,0:T(8,128)}, u32[]{:S(2)}) copy-start(f32[256,128]{1,0:T(8,128)} %param.21) | copy-start | bytes 393220
  15.9 159.2 %all-gather.7.cloned.1.call-start = ((), (), s32[]{:S(2)}) async-start(), calls=%async_computation.1 | async-start | bytes 2162688 | tf_op jit(solution)/shard_map/all_gather | solution.py:25
  177.1 34.8 %copy-start.7 = (f32[256,128]{1,0:T(8,128)}, f32[256,128]{1,0:T(8,128)S(1)}, u32[]{:S(2)}) copy-start(f32[256,128]{1,0:T(8,128)S(1)} %get-tuple-element.26) | copy-start | bytes 393220
  177.1 34.8 %copy-start.8 = (f32[256,128]{1,0:T(8,128)}, f32[256,128]{1,0:T(8,128)S(1)}, u32[]{:S(2)}) copy-start(f32[256,128]{1,0:T(8,128)S(1)} %get-tuple-element.27) | copy-start | bytes 393220
  177.1 34.8 %copy-start.9 = (f32[256,128]{1,0:T(8,128)}, f32[256,128]{1,0:T(8,128)S(1)}, u32[]{:S(2)}) copy-start(f32[256,128]{1,0:T(8,128)S(1)} %get-tuple-element.32) | copy-start | bytes 393220
  177.1 34.8 %copy-start.10 = (f32[256,128]{1,0:T(8,128)}, f32[256,128]{1,0:T(8,128)S(1)}, u32[]{:S(2)}) copy-start(f32[256,128]{1,0:T(8,128)S(1)} %get-tuple-element.33) | copy-start | bytes 393220
Sparse Core Ops, SparseCore 0:
  16.0 84.1 all-gather.4
  103.5 71.5 all-gather.6
where the time goes:
time: 219 us
  blocking collectives  104 us (47%)
  waiting for transfers between devices  78.7 us (36%)
  between operations  15.6 us (7%)
  matrix products  13.2 us (6%)
  other arithmetic  4.46 us (2%)
  local copies, waits for them, and re-layouts  2.82 us (1%)
    all_gather x2, waiting for transfers between devices, total_of_pieces(): pieces = lax.all_gather(array, axis).astype(jnp.float32)  78.6 us
    psum x4, blocking collectives, over_axes(): return functools.reduce(lax.psum, axes, array)  73.1 us
    all_gather x1, blocking collectives, sent_together(): result, at, done = (lax.all_gather(both, axis, axis=dim, tiled=True), 0, [])  30.8 us
    dot_general x2, matrix products, contract_rows(): return jnp.dot(left.T, right, precision=lax.Precision.HIGHEST)  5.1 us
    dot_general x1, matrix products, body(): reduced = jnp.dot(latent, factors, preferred_element_type=jnp.float32)  4.96 us
  transfers between devices with their start and end apart: 2, of which 2 were waited for; matrix products, arithmetic and copies ran while one was open for 3% of the time, Pallas kernels for 0%

commit v1 on v0

v1 whole, which is shorter than its diff:
```python
import jax
import jax.numpy as jnp
from jax import lax
from jax.experimental import pallas as pl
from jax.experimental.pallas import tpu as pltpu
from jax.sharding import Mesh
from jax.sharding import PartitionSpec as P

Z, CORE = "fs_0", "fs_1"
FS = (Z, CORE)
TP = ("tp_0", "tp_1")

EPSILON = 1e-08
FIRST_DECAY = 0.7
SECOND_DECAY = 0.8
LEARN_RATE = 0.2

BF16, F32 = jnp.bfloat16, jnp.float32


def halves(x):
    high = x.astype(BF16)
    return high, (x - high.astype(F32)).astype(BF16)


def thirds(x):
    high = x.astype(BF16)
    rest = x - high.astype(F32)
    return (high,) + halves(rest)


def squares_kernel(key_ref, value_ref, out_ref):
    totals = [jnp.sum(r[...] * r[...]) for r in (key_ref, value_ref)]
    row = lax.broadcasted_iota(jnp.int32, out_ref.shape, 1)
    out_ref[...] = jnp.where(row == 0, totals[0], totals[1])


def project_kernel(core_ref, latent_ref, key_ref, value_ref, key_proj, value_proj, keep_ref, send_ref, acc_ref):
    step = pl.program_id(0)
    both = jnp.concatenate([key_ref[...], value_ref[...]], axis=1)
    part = lax.dot_general(both, latent_ref[...], (((0,), (0,)), ((), ())), preferred_element_type=F32)

    @pl.when(step == 0)
    def _():
        acc_ref[...] = part

    @pl.when(step > 0)
    def _():
        acc_ref[...] += part

    @pl.when(step == pl.num_programs(0) - 1)
    def _():
        results = []
        cols = key_ref.shape[1]
        for at, proj in ((0, key_proj), (cols, value_proj)):
            high, low = halves(acc_ref[at : at + cols, :])
            p = proj[...]
            r = jnp.dot(high, p, preferred_element_type=F32) + jnp.dot(low, p, preferred_element_type=F32)
            results.append(r.T)
        first = core_ref[0] == 0
        keep_ref[...] = jnp.where(first, results[0], results[1])
        send_ref[...] = jnp.where(first, results[1], results[0]).astype(BF16)


def spread_kernel(pieces_ref, key_ref, value_ref, squares_ref, out_ref):
    rows = pieces_ref.shape[1]
    total = jnp.sum(pieces_ref[...].astype(F32), axis=0).astype(BF16)
    squares = jnp.sum(squares_ref[...], axis=0)
    scalars = [t[0:1] for t in thirds(squares)] + [t[1:2] for t in thirds(squares)]
    scalars += [jnp.zeros((2, total.shape[1]), BF16)]
    message = jnp.concatenate(
        [total, key_ref[...].astype(BF16), value_ref[...].astype(BF16)], axis=0
    )
    tail = jnp.concatenate([s.astype(F32) for s in scalars], axis=0).astype(BF16)
    at = message.shape[0]
    for i in range(out_ref.shape[0]):
        out_ref[i, :at] = message
        out_ref[i, at:] = tail


def update_kernel(
    place_ref, data_ref, key_w, value_w, key_proj, value_proj, kf, ks, vf, vs,
    key_renewed, value_renewed, key_step, value_step,
    kf_new, ks_new, vf_new, vs_new, key_copy, value_copy,
    *, rows, weight_rows, entries,
):
    own = pl.multiple_of(place_ref[0] * weight_rows, weight_rows)
    cores, chips = data_ref.shape[0], data_ref.shape[1]
    tail = rows + 2 * weight_rows
    for which, (w, proj, first, second, renewed, step, first_new, second_new, copy) in enumerate((
        (key_w, key_proj, kf, ks, key_renewed, key_step, kf_new, ks_new, key_copy),
        (value_w, value_proj, vf, vs, value_renewed, value_step, vf_new, vs_new, value_copy),
    )):
        projected = data_ref[which, :, :rows, :].reshape(chips * rows, w.shape[1]).astype(F32)
        fn = FIRST_DECAY * first[...] + (1.0 - FIRST_DECAY) * projected
        sn = SECOND_DECAY * second[...] + (1.0 - SECOND_DECAY) * projected * projected
        first_new[...] = fn
        second_new[...] = sn
        pair = jnp.concatenate(halves(fn / (jnp.sqrt(sn) + EPSILON)), axis=1)
        sums = data_ref[:, :, tail:, :].astype(F32).sum(axis=(0, 1))
        total = sums[3 * which : 3 * which + 1] + sums[3 * which + 1 : 3 * which + 2] + sums[3 * which + 2 : 3 * which + 3]
        scale = LEARN_RATE * jnp.sqrt(total / entries)
        cols = w.shape[1]

        def steps_of(factor):
            r = jnp.dot(factor, pair, preferred_element_type=F32)
            return scale * (r[:, :cols] + r[:, cols:])

        mine = steps_of(proj[pl.ds(own, weight_rows), :])
        step[...] = mine
        renewed[...] = w[...] - mine
        everyone = steps_of(proj[...])
        at = rows + which * weight_rows
        for chip in range(chips):
            for core in range(cores):
                r = (chip * cores + core) * weight_rows
                old = data_ref[core, chip, at : at + weight_rows, :].astype(F32)
                copy[r : r + weight_rows, :] = (old - everyone[r : r + weight_rows]).astype(BF16)


def whole(a):
    return pl.BlockSpec(memory_space=pltpu.VMEM)


def body(
    latent, key_cotangent, value_cotangent, key_weight, value_weight,
    key_projector, value_projector, key_first, key_second, value_first, value_second,
):
    chips, cores = lax.axis_size(Z), lax.axis_size(CORE)
    columns = lax.axis_size(TP)
    weight_rows, cols = key_weight.shape
    tokens, width = latent.shape
    rank = key_projector.shape[1]
    core = lax.axis_index(CORE).astype(jnp.int32)
    place = lax.axis_index(FS).astype(jnp.int32)
    sds = jax.ShapeDtypeStruct
    smem = pl.BlockSpec(memory_space=pltpu.SMEM)
    vmem = pl.BlockSpec(memory_space=pltpu.VMEM)

    squares = pl.pallas_call(
        squares_kernel, out_shape=sds((columns, 8, 128), F32),
        in_specs=[vmem, vmem], out_specs=vmem, name="squares",
    )(key_weight, value_weight)
    squares = lax.all_to_all(squares, TP, 0, 0)

    block = min(tokens, 512)
    keep, send = pl.pallas_call(
        project_kernel,
        grid=(tokens // block,),
        out_shape=(sds((rank, cols), F32), sds((rank, cols), BF16)),
        in_specs=[
            smem,
            pl.BlockSpec((block, width), lambda i: (i, 0)),
            pl.BlockSpec((block, cols), lambda i: (i, 0)),
            pl.BlockSpec((block, cols), lambda i: (i, 0)),
            pl.BlockSpec((width, rank), lambda i: (0, 0)),
            pl.BlockSpec((width, rank), lambda i: (0, 0)),
        ],
        out_specs=(pl.BlockSpec((rank, cols), lambda i: (0, 0)),) * 2,
        scratch_shapes=[pltpu.VMEM((2 * cols, width), F32)],
        cost_estimate=pl.CostEstimate(flops=2_000_000_000, bytes_accessed=6_000_000, transcendentals=0),
        name="project",
    )(core.reshape(1), latent, key_cotangent, value_cotangent, key_projector, value_projector)

    other = lax.ppermute(send, CORE, [(0, 1), (1, 0)])
    rows = rank // chips
    pieces = (keep + other.astype(F32)).astype(BF16).reshape(chips, rows, cols)
    pieces = lax.all_to_all(pieces, Z, 0, 0)

    length = rows + 2 * weight_rows + 8
    message = pl.pallas_call(
        spread_kernel, out_shape=sds((chips, length, cols), BF16),
        in_specs=[vmem] * 4, out_specs=vmem, name="spread",
    )(pieces, key_weight, value_weight, squares)
    message = lax.all_to_all(message, Z, 0, 0)
    data = lax.all_gather(message, CORE)

    entries = float(key_weight.size * chips * cores * columns)
    weight = sds((weight_rows, cols), F32)
    moment = sds((rank, cols), F32)
    copy = sds((width, cols), BF16)

    def update(*refs):
        update_kernel(*refs, rows=rows, weight_rows=weight_rows, entries=entries)

    return pl.pallas_call(
        update,
        out_shape=(weight,) * 4 + (moment,) * 4 + (copy,) * 2,
        in_specs=[smem] + [vmem] * 9, out_specs=(vmem,) * 10, name="update",
    )(
        place.reshape(1), data, key_weight, value_weight, key_projector, value_projector,
        key_first, key_second, value_first, value_second,
    )


def solution(mesh):
    finer = Mesh(mesh.devices.reshape(16, 2, 8, 4), ("fs_0", "fs_1", "tp_0", "tp_1"))
    return jax.shard_map(
        body,
        mesh=finer,
        in_specs=(P(FS, None),) + (P(FS, TP),) * 4 + (P(),) * 2 + (P(None, TP),) * 4,
        out_specs=(P(FS, TP),) * 4 + (P(None, TP),) * 6,
        check_vma=False,
    )
```

time: 219 us -> 95.1 us (0.43)
  blocking collectives: 104 us -> 34 us
  waiting for transfers between devices: 78.7 us -> 23.2 us
  starting transfers between devices: 0.08 us -> 23.4 us
  between operations: 15.6 us -> 0.7 us
  matrix products: 13.2 us -> 0 us
  Pallas kernels: 0 us -> 12.3 us
  other arithmetic: 4.46 us -> 0.92 us
  local copies, waits for them, and re-layouts: 2.82 us -> 0.01 us
    all_gather x2 -> x0, waiting for transfers between devices: 78.6 us -> none  [total_of_pieces(): pieces = lax.all_gather(array, axis).astype(jnp.float32)]
    psum x4 -> x0, blocking collectives: 73.1 us -> none  [over_axes(): return functools.reduce(lax.psum, axes, array)]
    all_to_all x0 -> x1, blocking collectives: none -> 23.3 us  [body(): pieces = lax.all_to_all(pieces, Z, 0, 0)]
    all_to_all x0 -> x2, waiting for transfers between devices: none -> 23.2 us  [the longest x1 14.3 us: body(): message = lax.all_to_all(message, Z, 0, 0)]
    all_gather x1, blocking collectives: 30.8 us -> 10.7 us  [body(): data = lax.all_gather(message, CORE)]
    ppermute x0 -> x1, starting transfers between devices: none -> 16 us  [body(): other = lax.ppermute(send, CORE, [(0, 1), (1, 0)])]
    dot_general x5 -> x0, matrix products: 13.2 us -> none  [the longest x2 5.1 us: contract_rows(): return jnp.dot(left.T, right, precision=lax.Precision.HIGHEST)]
    pallas_call x0 -> x4, Pallas kernels: none -> 12.3 us  [the longest x1 5.96 us: body(): pl.pallas_call(project_kernel, grid=(tokens // block,), out_shape=(sds((r...]
  transfers between devices with their start and end apart: 2 -> 3, of which waited for: 2 -> 2; matrix products, arithmetic and copies ran while one was open for 3% -> 1% of each run, Pallas kernels for 0% -> 2%
where the time goes in v1:
time: 95.1 us; the launch traced here: 94.6 us
  blocking collectives  34 us (36%)
  starting transfers between devices  23.4 us (25%)
  waiting for transfers between devices  23.2 us (24%)
  Pallas kernels  12.3 us (13%)
    all_to_all x1, blocking collectives, body(): pieces = lax.all_to_all(pieces, Z, 0, 0)  23.3 us
    ppermute x1, starting transfers between devices, body(): other = lax.ppermute(send, CORE, [(0, 1), (1, 0)])  16 us
    all_to_all x1, waiting for transfers between devices, body(): message = lax.all_to_all(message, Z, 0, 0)  14.3 us
    all_gather x1, blocking collectives, body(): data = lax.all_gather(message, CORE)  10.7 us
    all_to_all x1, waiting for transfers between devices, body(): squares = lax.all_to_all(squares, TP, 0, 0)  8.92 us
    pallas_call x1, Pallas kernels, body(): pl.pallas_call(project_kernel, grid=(tokens // block,), out_shape=(sds((r...  5.96 us
    all_to_all x1, starting transfers between devices, body(): squares = lax.all_to_all(squares, TP, 0, 0)  3.86 us
    all_to_all x1, starting transfers between devices, body(): message = lax.all_to_all(message, Z, 0, 0)  3.55 us
  transfers between devices with their start and end apart: 3, of which 2 were waited for; matrix products, arithmetic and copies ran while one was open for 1% of the time, Pallas kernels for 2%

profile of v1, /device:TPU:1, one launch (start us, length us, event | category | flops | bytes accessed | tf_op | source)
XLA Modules:
  0.0 94.6 jit_solution(5486726201263184188)
XLA Ops:
  0.6 6.0 %project.1 = (f32[256,128]{1,0:T(8,128)}, bf16[256,128]{1,0:T(8,128)(2,1)}) custom-call(s32[1]{0:T(128)} %bitcast.1.core_ref, bf16[2048,1024]{1,0:T(8,128)(2,1)} %latent_ref.1, bf16[2048,128]{1,0:T(8,128)(2,1)} %key_ref.3, bf16[2048,128]{1,0:T(8,128)(2,1)} %value_ref.3, bf16[1024,256]{1,0:T(8,128)(2,1)} %refs_4_.1, bf16[1024,256]{1,0:T(8,128)(2,1)} %refs_5_.1), custom_call_target="tpu_custom_call" | custom-call | flops 2000000000 | bytes 6000000 | tf_op jit(solution)/shard_map/project/pallas_call | solution.py:147
  6.6 16.0 %collective-permute-start = (bf16[256,128]{1,0:T(8,128)(2,1)}, bf16[256,128]{1,0:T(8,128)(2,1)S(1)}, u32[]{:S(2)}, u32[]{:S(2)}) collective-permute-start(bf16[256,128]{1,0:T(8,128)(2,1)} %get-tuple-element.13), channel_id=1, source_target_pairs={{0,32},{32,0},{1,33},{33,1},{2,34},{34,2},{3,35},{35,3},{4,36},{36... | collective-permute-start | bytes 196616 | tf_op jit(solution)/shard_map/ppermute | solution.py:165
  22.6 1.5 %squares.1 = f32[32,8,128]{2,1,0:T(8,128)} custom-call(f32[32,128]{1,0:T(8,128)} %refs_2_.1, f32[32,128]{1,0:T(8,128)} %refs_3_.1), custom_call_target="tpu_custom_call" | custom-call | tf_op jit(solution)/shard_map/squares/pallas_call | solution.py:140
  24.1 3.9 %all-to-all-start.1 = ((f32[32,8,128]{2,1,0:T(8,128)}), f32[32,8,128]{2,1,0:T(8,128)S(1)}, u32[]{:S(2)}, u32[]{:S(2)}) async-start(f32[32,8,128]{2,1,0:T(8,128)} %squares.1), calls=%async_computation.1 | async-start | bytes 262144 | tf_op jit(solution)/shard_map/all_to_all | solution.py:144
  28.0 0.0 collective-permute-done
  28.0 0.9 add_convert_fusion
  29.0 8.9 %all-to-all-done.1.squares_ref = f32[32,8,128]{2,1,0:T(8,128)S(1)} async-done(((f32[32,8,128]{2,1,0:T(8,128)}), f32[32,8,128]{2,1,0:T(8,128)S(1)}, u32[]{:S(2)}, u32[]{:S(2)}) %all-to-all-start.1) | async-done | bytes 131104 | tf_op jit(solution)/shard_map/all_to_all | solution.py:144
  37.9 0.0 copy-start
  37.9 23.3 %all_to_all.15.pieces_ref = bf16[16,16,128]{2,1,0:T(8,128)(2,1)} all-to-all(bf16[16,16,128]{2,1,0:T(8,128)(2,1)S(1)} %bitcast.5), channel_id=1, replica_groups=mesh['fs_0'=16,'fs_1'=2,'tp_0'=8,'tp_1'=4] {'fs_0'}, dimensions={0} | all-to-all | bytes 131072 | tf_op jit(solution)/shard_map/all_to_all | solution.py:168
  61.2 0.0 copy-done
  61.2 1.8 %spread.1 = bf16[16,88,128]{2,1,0:T(8,128)(2,1)} custom-call(bf16[16,16,128]{2,1,0:T(8,128)(2,1)} %all_to_all.15.pieces_ref, f32[32,128]{1,0:T(8,128)} %refs_2_.1, f32[32,128]{1,0:T(8,128)} %refs_3_.1, f32[32,8,128]{2,1,0:T(8,128)} %copy-done), custom_call_target="tpu_custom_call" | custom-call | tf_op jit(solution)/shard_map/spread/pallas_call | solution.py:171
  62.9 3.5 %all-to-all-start.2 = ((bf16[16,88,128]{2,1,0:T(8,128)(2,1)}), bf16[16,88,128]{2,1,0:T(8,128)(2,1)S(1)}, u32[]{:S(2)}, u32[]{:S(2)}) async-start(bf16[16,88,128]{2,1,0:T(8,128)(2,1)} %spread.1), calls=%async_computation.2 | async-start | bytes 720896 | tf_op jit(solution)/shard_map/all_to_all | solution.py:175
  66.5 14.3 %all-to-all-done.2 = bf16[16,88,128]{2,1,0:T(8,128)(2,1)S(1)} async-done(((bf16[16,88,128]{2,1,0:T(8,128)(2,1)}), bf16[16,88,128]{2,1,0:T(8,128)(2,1)S(1)}, u32[]{:S(2)}, u32[]{:S(2)}) %all-to-all-start.2) | async-done | bytes 360480 | tf_op jit(solution)/shard_map/all_to_all | solution.py:175
  80.8 10.7 %all-gather = bf16[32,88,128]{2,1,0:T(8,128)(2,1)} all-gather(bf16[16,88,128]{2,1,0:T(8,128)(2,1)S(1)} %all-to-all-done.2), channel_id=2, replica_groups=mesh['fs_0'=16,'fs_1'=2,'tp_0'=8,'tp_1'=4] {'fs_1'}, dimensions={0}, use_global_device_ids=true | all-gather | bytes 1081344 | tf_op jit(solution)/shard_map/all_gather | solution.py:176
  91.6 3.0 %update.1 = (f32[32,128]{1,0:T(8,128)}, f32[32,128]{1,0:T(8,128)}, f32[32,128]{1,0:T(8,128)}, f32[32,128]{1,0:T(8,128)}, f32[256,128]{1,0:T(8,128)}, /*index=5*/...) custom-call(s32[1]{0:T(128)} %bitcast.refs_0_, ...), custom_call_target="tpu_custom_call" | custom-call | tf_op jit(solution)/shard_map/update/pallas_call | solution.py:186
Async XLA Ops:
  6.6 21.4 %collective-permute-start = (bf16[256,128]{1,0:T(8,128)(2,1)}, bf16[256,128]{1,0:T(8,128)(2,1)S(1)}, u32[]{:S(2)}, u32[]{:S(2)}) collective-permute-start(bf16[256,128]{1,0:T(8,128)(2,1)} %get-tuple-element.13), channel_id=1, source_target_pairs={{0,32},{32,0},{1,33},{33,1},{2,34},{34,2},{3,35},{35,3},{4,36},{36... | collective-permute-start | bytes 196616 | tf_op jit(solution)/shard_map/ppermute | solution.py:165
  24.1 13.7 %all-to-all-start.1 = ((f32[32,8,128]{2,1,0:T(8,128)}), f32[32,8,128]{2,1,0:T(8,128)S(1)}, u32[]{:S(2)}, u32[]{:S(2)}) async-start(f32[32,8,128]{2,1,0:T(8,128)} %squares.1), calls=%async_computation.1 | async-start | bytes 262144 | tf_op jit(solution)/shard_map/all_to_all | solution.py:144
  37.9 23.3 %copy-start = (f32[32,8,128]{2,1,0:T(8,128)}, f32[32,8,128]{2,1,0:T(8,128)S(1)}, u32[]{:S(2)}) copy-start(f32[32,8,128]{2,1,0:T(8,128)S(1)} %all-to-all-done.1.squares_ref) | copy-start | bytes 393220
  62.9 17.9 %all-to-all-start.2 = ((bf16[16,88,128]{2,1,0:T(8,128)(2,1)}), bf16[16,88,128]{2,1,0:T(8,128)(2,1)S(1)}, u32[]{:S(2)}, u32[]{:S(2)}) async-start(bf16[16,88,128]{2,1,0:T(8,128)(2,1)} %spread.1), calls=%async_computation.2 | async-start | bytes 720896 | tf_op jit(solution)/shard_map/all_to_all | solution.py:175

commit v2 on v1

v2 whole, which is shorter than its diff:
```python
import jax
import jax.numpy as jnp
from jax import lax
from jax.experimental import pallas as pl
from jax.experimental.pallas import tpu as pltpu
from jax.sharding import Mesh
from jax.sharding import PartitionSpec as P


Z, CORE = "fs_0", "fs_1"
FS = (Z, CORE)
TP = ("tp_0", "tp_1")

EPSILON = 1e-08
FIRST_DECAY = 0.7
SECOND_DECAY = 0.8
LEARN_RATE = 0.2
LEAD = 0
TAIL = 8

BF16, F32 = jnp.bfloat16, jnp.float32


def halves(x):
    high = x.astype(BF16)
    return high, (x - high.astype(F32)).astype(BF16)


def tail_of(x, cols):
    row = lax.broadcasted_iota(jnp.int32, (TAIL, cols), 0)
    x = jnp.broadcast_to(x, (TAIL, cols))
    high = x.astype(BF16).astype(F32)
    mid = (x - high).astype(BF16).astype(F32)
    low = x - high - mid
    x = jnp.where(row == 0, high, jnp.where(row == 1, mid, jnp.where(row == 2, low, 0.0)))
    return x.astype(BF16)


def squares_kernel(key_ref, value_ref, out_ref):
    row = lax.broadcasted_iota(jnp.int32, out_ref.shape, 1)
    out_ref[...] = jnp.where(row == 0, jnp.sum(key_ref[...] * key_ref[...]), jnp.sum(value_ref[...] * value_ref[...]))


def project_kernel(
    latent_hbm, key_hbm, value_hbm, key_proj_hbm, value_proj_hbm, out_ref,
    latent, key, value, key_proj, value_proj, acc_ref, sems,
):
    chunks = sems.shape[0] - 4
    tokens = latent.shape[0] // chunks
    cols = key.shape[1]
    sides = [
        pltpu.make_async_copy(src, dst, sems.at[chunks + i])
        for i, (src, dst) in enumerate((
            (key_hbm, key), (value_hbm, value), (key_proj_hbm, key_proj), (value_proj_hbm, value_proj)
        ))
    ]
    mains = [
        pltpu.make_async_copy(
            latent_hbm.at[pl.ds(i * tokens, tokens)], latent.at[pl.ds(i * tokens, tokens)], sems.at[i]
        )
        for i in range(chunks)
    ]
    for copy in sides[:2] + mains + sides[2:]:
        copy.start()
    sides[0].wait()
    sides[1].wait()
    for i in range(chunks):
        mains[i].wait()
        at = slice(i * tokens, (i + 1) * tokens)
        both = jnp.concatenate([key[at, :], value[at, :]], axis=1)
        part = lax.dot_general(both, latent[at, :], (((0,), (0,)), ((), ())), preferred_element_type=F32)
        acc_ref[...] = part if i == 0 else acc_ref[...] + part
    for which, proj in enumerate((key_proj, value_proj)):
        sides[2 + which].wait()
        high, low = halves(acc_ref[which * cols : (which + 1) * cols])
        p = proj[...]
        r = jnp.dot(high, p, preferred_element_type=F32) + jnp.dot(low, p, preferred_element_type=F32)
        out_ref[which] = r.T.astype(BF16)


def cut_kernel(core_ref, parts_ref, squares_ref, out_ref):
    chips, length, cols = out_ref.shape
    rows = length - TAIL
    mine = parts_ref[:, core_ref[0]].astype(F32).sum(axis=0)
    out_ref[:, :rows] = mine.astype(BF16).reshape(chips, rows, cols)
    squares = jnp.sum(squares_ref[...], axis=0)
    row = lax.broadcasted_iota(jnp.int32, (TAIL, cols), 0)
    key = tail_of(squares[0:1], cols).astype(F32)
    value = tail_of(squares[1:2], cols).astype(F32)
    tail = jnp.where(row < TAIL // 2, key, pltpu.roll(value, TAIL // 2, 0)).astype(BF16)
    for i in range(chips):
        out_ref[i, rows:] = tail


def spread_kernel(pieces_ref, key_ref, value_ref, out_ref, squares_ref):
    rows = pieces_ref.shape[1] - TAIL
    total = jnp.sum(pieces_ref[...].astype(F32), axis=0)
    message = jnp.concatenate(
        [total[:rows].astype(BF16), key_ref[...].astype(BF16), value_ref[...].astype(BF16)], axis=0
    )
    for i in range(out_ref.shape[0]):
        out_ref[i] = message
    key = total[rows : rows + 1] + total[rows + 1 : rows + 2] + total[rows + 2 : rows + 3]
    rows += TAIL // 2
    value = total[rows : rows + 1] + total[rows + 1 : rows + 2] + total[rows + 2 : rows + 3]
    row = lax.broadcasted_iota(jnp.int32, squares_ref.shape, 0)
    squares_ref[...] = jnp.where(row == 0, key, value)


def update_kernel(
    place_ref, data_ref, squares_ref, key_w, value_w, key_proj, value_proj, kf, ks, vf, vs,
    key_renewed, value_renewed, key_step, value_step,
    kf_new, ks_new, vf_new, vs_new, key_copy, value_copy,
    *, rows, weight_rows, entries,
):
    own = pl.multiple_of(place_ref[0] * weight_rows, weight_rows)
    cores, chips = data_ref.shape[0], data_ref.shape[1]
    squares = squares_ref[...]
    for which, (w, proj, first, second, renewed, step, first_new, second_new, copy) in enumerate((
        (key_w, key_proj, kf, ks, key_renewed, key_step, kf_new, ks_new, key_copy),
        (value_w, value_proj, vf, vs, value_renewed, value_step, vf_new, vs_new, value_copy),
    )):
        projected = data_ref[which, :, :rows, :].reshape(chips * rows, w.shape[1]).astype(F32)
        fn = FIRST_DECAY * first[...] + (1.0 - FIRST_DECAY) * projected
        sn = SECOND_DECAY * second[...] + (1.0 - SECOND_DECAY) * projected * projected
        first_new[...] = fn
        second_new[...] = sn
        pair = jnp.concatenate(halves(fn / (jnp.sqrt(sn) + EPSILON)), axis=1)
        total = squares[which : which + 1]
        scale = LEARN_RATE * jnp.sqrt(total / entries)
        cols = w.shape[1]

        def steps_of(factor):
            r = jnp.dot(factor, pair, preferred_element_type=F32)
            return scale * (r[:, :cols] + r[:, cols:])

        mine = steps_of(proj[pl.ds(own, weight_rows), :])
        step[...] = mine
        renewed[...] = w[...] - mine
        everyone = steps_of(proj[...])
        at = rows + which * weight_rows
        for chip in range(chips):
            for core in range(cores):
                r = ((chip + LEAD) % chips * cores + core) * weight_rows
                old = data_ref[core, chip, at : at + weight_rows, :].astype(F32)
                copy[r : r + weight_rows, :] = (old - everyone[r : r + weight_rows]).astype(BF16)


def swap(a, chips):
    if LEAD == 0:
        return lax.all_to_all(a, Z, 0, 0)
    order = [(i + LEAD) % chips for i in range(chips)]
    return lax.all_to_all(a, Z, 0, 0, axis_index_groups=[order])


def near(a):
    return pltpu.with_memory_space_constraint(a, pltpu.VMEM)


def body(
    latent, key_cotangent, value_cotangent, key_weight, value_weight,
    key_projector, value_projector, key_first, key_second, value_first, value_second,
):
    chips, cores = lax.axis_size(Z), lax.axis_size(CORE)
    columns = lax.axis_size(TP)
    weight_rows, cols = key_weight.shape
    tokens, width = latent.shape
    rank = key_projector.shape[1]
    core = lax.axis_index(CORE).astype(jnp.int32)
    place = lax.axis_index(FS).astype(jnp.int32)
    sds = jax.ShapeDtypeStruct
    smem = pl.BlockSpec(memory_space=pltpu.SMEM)
    vmem = pl.BlockSpec(memory_space=pltpu.VMEM)

    squares = pl.pallas_call(
        squares_kernel, out_shape=(sds((cores * lax.axis_size(TP[1]), 8, cols), F32),),
        in_specs=[vmem, vmem], out_specs=(vmem,), name="squares",
    )(key_weight, value_weight)[0]
    squares = lax.all_to_all(squares, (CORE, TP[1]), 0, 0)
    parts = pl.pallas_call(
        project_kernel,
        out_shape=(pltpu.VMEM((2, rank, cols), BF16),),
        in_specs=[pl.BlockSpec(memory_space=pl.ANY)] * 5,
        out_specs=(vmem,),
        scratch_shapes=[
            pltpu.VMEM(latent.shape, BF16),
            pltpu.VMEM((tokens, cols), BF16),
            pltpu.VMEM((tokens, cols), BF16),
            pltpu.VMEM((width, rank), BF16),
            pltpu.VMEM((width, rank), BF16),
            pltpu.VMEM((2 * cols, width), F32),
            pltpu.SemaphoreType.DMA((8 + 4,)),
        ],
        name="project",
    )(latent, key_cotangent, value_cotangent, key_projector, value_projector)[0]
    parts = near(lax.all_gather(parts, CORE))

    rows = rank // chips
    pieces = pl.pallas_call(
        cut_kernel, out_shape=(pltpu.VMEM((chips, rows + TAIL, cols), BF16),),
        in_specs=[smem, vmem, vmem], out_specs=(vmem,), name="cut",
    )(core.reshape(1), parts, near(squares))[0]
    pieces = near(swap(pieces, chips))

    length = rows + 2 * weight_rows
    message, squares = pl.pallas_call(
        spread_kernel,
        out_shape=(pltpu.VMEM((chips, length, cols), BF16), pltpu.VMEM((8, cols), F32)),
        in_specs=[vmem] * 3, out_specs=(vmem, vmem), name="spread",
    )(pieces, near(key_weight), near(value_weight))
    message = swap(message, chips)
    squares = lax.psum(squares, TP[0])
    data = near(lax.all_gather(message, CORE))

    entries = float(key_weight.size * chips * cores * columns)
    weight = sds((weight_rows, cols), F32)
    moment = sds((rank, cols), F32)
    copy = sds((width, cols), BF16)

    def update(*refs):
        update_kernel(*refs, rows=rows, weight_rows=weight_rows, entries=entries)

    return pl.pallas_call(
        update,
        out_shape=(weight,) * 4 + (moment,) * 4 + (copy,) * 2,
        in_specs=[smem] + [vmem] * 10, out_specs=(vmem,) * 10, name="update",
    )(
        place.reshape(1), data, near(squares), *map(near, (
            key_weight, value_weight, key_projector, value_projector,
            key_first, key_second, value_first, value_second,
        ))
    )


def solution(mesh):
    finer = Mesh(mesh.devices.reshape(16, 2, 8, 4), ("fs_0", "fs_1", "tp_0", "tp_1"))
    return jax.shard_map(
        body,
        mesh=finer,
        in_specs=(P(FS, None),) + (P(FS, TP),) * 4 + (P(),) * 2 + (P(None, TP),) * 4,
        out_specs=(P(FS, TP),) * 4 + (P(None, TP),) * 6,
        check_vma=False,
    )
```

time: 95.1 us -> 76.3 us (0.80)
  waiting for transfers between devices: 23.2 us -> 1.16 us
  blocking collectives: 34 us -> 43.3 us
  Pallas kernels: 12.3 us -> 8.1 us
    all_to_all x2, waiting for transfers between devices: 23.2 us -> 1.16 us  [the longest x1 1.16 us: swap(): return lax.all_to_all(a, Z, 0, 0)]
    ppermute x1 -> x0, starting transfers between devices: 16 us -> none  [body(): other = lax.ppermute(send, CORE, [(0, 1), (1, 0)])]
    all_to_all x2, starting transfers between devices: 7.41 us -> 22.6 us  [the longest x1 17.4 us: body(): squares = lax.all_to_all(squares, (CORE, TP[1]), 0, 0)]
    psum x0 -> x1, blocking collectives: none -> 14.2 us  [body(): squares = lax.psum(squares, TP[0])]
    all_to_all x1, blocking collectives: 23.3 us -> 18.7 us  [swap(): return lax.all_to_all(a, Z, 0, 0)]
    pallas_call x3 -> x4, Pallas kernels: 9.25 us -> 6.65 us  [the longest x1 4.33 us: body(): pl.pallas_call(project_kernel, out_shape=(pltpu.VMEM((2, rank, cols), BF1...]
    pallas_call x1, Pallas kernels: 3.02 us -> 1.45 us  [body(): pl.pallas_call(update, out_shape=(weight,) * 4 + (moment,) * 4 + (copy,)...]
    all_gather x1 -> x2, blocking collectives: 10.7 us -> 10.4 us  [the longest x1 8.38 us: body(): data = near(lax.all_gather(message, CORE))]
  transfers between devices with their start and end apart: 3 -> 2, of which waited for: 2 -> 1; matrix products, arithmetic and copies ran while one was open for 1% -> 0% of each run, Pallas kernels for 2% -> 6%
where the time goes in v2:
time: 76.3 us; the launch traced here: 75.9 us
  blocking collectives  43.3 us (57%)
  starting transfers between devices  22.6 us (30%)
  Pallas kernels  8.1 us (11%)
  waiting for transfers between devices  1.16 us (2%)
    all_to_all x1, blocking collectives, swap(): return lax.all_to_all(a, Z, 0, 0)  18.7 us
    all_to_all x1, starting transfers between devices, body(): squares = lax.all_to_all(squares, (CORE, TP[1]), 0, 0)  17.4 us
    psum x1, blocking collectives, body(): squares = lax.psum(squares, TP[0])  14.2 us
    all_gather x1, blocking collectives, body(): data = near(lax.all_gather(message, CORE))  8.38 us
    all_to_all x1, starting transfers between devices, swap(): return lax.all_to_all(a, Z, 0, 0)  5.2 us
    pallas_call x1, Pallas kernels, body(): pl.pallas_call(project_kernel, out_shape=(pltpu.VMEM((2, rank, cols), BF1...  4.33 us
    all_gather x1, blocking collectives, body(): parts = near(lax.all_gather(parts, CORE))  1.99 us
  transfers between devices with their start and end apart: 2, of which 1 were waited for; matrix products, arithmetic and copies ran while one was open for 0% of the time, Pallas kernels for 6%

profile of v2, /device:TPU:1, one launch (start us, length us, event | category | flops | bytes accessed | tf_op | source)
XLA Modules:
  0.0 75.9 jit_solution(3418335164406114247)
XLA Ops:
  0.6 0.0 copy-start.3
  0.7 0.0 copy-start.2
  0.7 1.5 %squares.1 = f32[8,8,128]{2,1,0:T(8,128)} custom-call(f32[32,128]{1,0:T(8,128)} %refs_3_.1, f32[32,128]{1,0:T(8,128)} %refs_4_.1), custom_call_target="tpu_custom_call" | custom-call | tf_op jit(solution)/shard_map/squares/pallas_call | solution.py:175
  2.2 17.4 %all-to-all-start = ((f32[8,8,128]{2,1,0:T(8,128)}), f32[8,8,128]{2,1,0:T(8,128)S(1)}, u32[]{:S(2)}, u32[]{:S(2)}) async-start(f32[8,8,128]{2,1,0:T(8,128)} %squares.1), calls=%async_computation | async-start | bytes 65536 | tf_op jit(solution)/shard_map/all_to_all | solution.py:179
  19.6 0.0 copy-start
  19.6 0.0 copy-start.1
  19.6 0.0 copy-start.4
  19.6 0.0 copy-start.5
  19.6 0.0 copy-start.6
  19.6 0.0 copy-start.7
  19.6 4.3 %project.1 = bf16[2,256,128]{2,1,0:T(8,128)(2,1)S(1)} custom-call(bf16[2048,1024]{1,0:T(8,128)(2,1)} %latent_hbm.1, bf16[2048,128]{1,0:T(8,128)(2,1)} %key_hbm.1, bf16[2048,128]{1,0:T(8,128)(2,1)} %value_hbm.1, bf16[1024,256]{1,0:T(8,128)(2,1)} %refs_5_.1, bf16[1024,256]{1,0:T(8,128)(2,1)} %refs_6_.1), custom_call_target="tpu_custom_call" | custom-call | tf_op jit(solution)/shard_map/project/pallas_call | solution.py:180
  23.9 2.0 %all-gather = bf16[4,256,128]{2,1,0:T(8,128)(2,1)S(1)} all-gather(bf16[2,256,128]{2,1,0:T(8,128)(2,1)S(1)} %project.1), channel_id=2, replica_groups=mesh['fs_0'=16,'fs_1'=2,'tp_0'=8,'tp_1'=4] {'fs_1'}, dimensions={0}, use_global_device_ids=true | all-gather | bytes 393216 | tf_op jit(solution)/shard_map/all_gather | solution.py:196
  25.9 0.0 all-to-all-done.squares_ref
  26.0 18.7 %all_to_all.15.pieces_ref = bf16[16,24,128]{2,1,0:T(8,128)(2,1)S(1)} all-to-all(bf16[16,24,128]{2,1,0:T(8,128)(2,1)S(1)} %cut.1), channel_id=1, replica_groups=mesh['fs_0'=16,'fs_1'=2,'tp_0'=8,'tp_1'=4] {'fs_0'}, dimensions={0} | all-to-all | bytes 196608 | tf_op jit(solution)/shard_map/all_to_all | solution.py:151
  44.7 0.0 copy-done.3
  44.7 0.0 copy-done.2
  44.7 0.8 spread.1
  45.5 5.2 %all-to-all-start.2 = ((bf16[16,80,128]{2,1,0:T(8,128)(2,1)}), bf16[16,80,128]{2,1,0:T(8,128)(2,1)S(1)}, u32[]{:S(2)}, u32[]{:S(2)}) async-start(bf16[16,80,128]{2,1,0:T(8,128)(2,1)} %get-tuple-element.12), calls=%async_computation.2 | async-start | bytes 655360 | tf_op jit(solution)/shard_map/all_to_all | solution.py:151
  50.7 14.2 %psum.7.refs_2_ = f32[8,128]{1,0:T(8,128)S(1)} all-reduce(f32[8,128]{1,0:T(8,128)S(1)} %get-tuple-element.13), channel_id=1, replica_groups=mesh['fs_0'=16,'fs_1'=2,'tp_0'=8,'tp_1'=4] {'tp_0'}, use_global_device_ids=true, to_apply=%region_0.0 | all-reduce | flops 1024 | bytes 8192 | tf_op jit(solution)/shard_map/psum | solution.py:212
  64.8 1.2 %all-to-all-done.2 = bf16[16,80,128]{2,1,0:T(8,128)(2,1)S(1)} async-done(((bf16[16,80,128]{2,1,0:T(8,128)(2,1)}), bf16[16,80,128]{2,1,0:T(8,128)(2,1)S(1)}, u32[]{:S(2)}, u32[]{:S(2)}) %all-to-all-start.2) | async-done | bytes 327712 | tf_op jit(solution)/shard_map/all_to_all | solution.py:151
  66.0 8.4 %all-gather.1 = bf16[32,80,128]{2,1,0:T(8,128)(2,1)S(1)} all-gather(bf16[16,80,128]{2,1,0:T(8,128)(2,1)S(1)} %all-to-all-done.2), channel_id=3, replica_groups=mesh['fs_0'=16,'fs_1'=2,'tp_0'=8,'tp_1'=4] {'fs_1'}, dimensions={0}, use_global_device_ids=true | all-gather | bytes 983040 | tf_op jit(solution)/shard_map/all_gather | solution.py:213
  74.4 0.0 copy-done
  74.4 0.0 copy-done.1
  74.4 0.0 copy-done.4
  74.4 0.0 copy-done.5
  74.4 0.0 copy-done.6
  74.4 0.0 copy-done.7
  74.4 1.5 %update.1 = (f32[32,128]{1,0:T(8,128)}, f32[32,128]{1,0:T(8,128)}, f32[32,128]{1,0:T(8,128)}, f32[32,128]{1,0:T(8,128)}, f32[256,128]{1,0:T(8,128)}, /*index=5*/...) custom-call(s32[1]{0:T(128)} %bitcast.refs_0_, ...), custom_call_target="tpu_custom_call" | custom-call | tf_op jit(solution)/shard_map/update/pallas_call | solution.py:223
  (1 shorter events, 0.0 us)
Async XLA Ops:
  0.6 44.1 %copy-start.3 = (f32[32,128]{1,0:T(8,128)S(1)}, f32[32,128]{1,0:T(8,128)}, u32[]{:S(2)}) copy-start(f32[32,128]{1,0:T(8,128)} %refs_4_.1) | copy-start | bytes 49156
  0.7 44.1 %copy-start.2 = (f32[32,128]{1,0:T(8,128)S(1)}, f32[32,128]{1,0:T(8,128)}, u32[]{:S(2)}) copy-start(f32[32,128]{1,0:T(8,128)} %refs_3_.1) | copy-start | bytes 49156
  2.2 23.8 %all-to-all-start = ((f32[8,8,128]{2,1,0:T(8,128)}), f32[8,8,128]{2,1,0:T(8,128)S(1)}, u32[]{:S(2)}, u32[]{:S(2)}) async-start(f32[8,8,128]{2,1,0:T(8,128)} %squares.1), calls=%async_computation | async-start | bytes 65536 | tf_op jit(solution)/shard_map/all_to_all | solution.py:179
  19.6 54.8 %copy-start = (bf16[1024,256]{1,0:T(8,128)(2,1)S(1)}, bf16[1024,256]{1,0:T(8,128)(2,1)}, u32[]{:S(2)}) copy-start(bf16[1024,256]{1,0:T(8,128)(2,1)} %refs_5_.1) | copy-start | bytes 1572868
  19.6 54.8 %copy-start.1 = (bf16[1024,256]{1,0:T(8,128)(2,1)S(1)}, bf16[1024,256]{1,0:T(8,128)(2,1)}, u32[]{:S(2)}) copy-start(bf16[1024,256]{1,0:T(8,128)(2,1)} %refs_6_.1) | copy-start | bytes 1572868
  19.6 54.8 %copy-start.4 = (f32[256,128]{1,0:T(8,128)S(1)}, f32[256,128]{1,0:T(8,128)}, u32[]{:S(2)}) copy-start(f32[256,128]{1,0:T(8,128)} %refs_7_.1) | copy-start | bytes 393220
  19.6 54.8 %copy-start.5 = (f32[256,128]{1,0:T(8,128)S(1)}, f32[256,128]{1,0:T(8,128)}, u32[]{:S(2)}) copy-start(f32[256,128]{1,0:T(8,128)} %refs_8_.1) | copy-start | bytes 393220
  19.6 54.8 %copy-start.6 = (f32[256,128]{1,0:T(8,128)S(1)}, f32[256,128]{1,0:T(8,128)}, u32[]{:S(2)}) copy-start(f32[256,128]{1,0:T(8,128)} %refs_9_.1) | copy-start | bytes 393220
  19.6 54.8 %copy-start.7 = (f32[256,128]{1,0:T(8,128)S(1)}, f32[256,128]{1,0:T(8,128)}, u32[]{:S(2)}) copy-start(f32[256,128]{1,0:T(8,128)} %refs_10_.1) | copy-start | bytes 393220
  45.5 20.5 %all-to-all-start.2 = ((bf16[16,80,128]{2,1,0:T(8,128)(2,1)}), bf16[16,80,128]{2,1,0:T(8,128)(2,1)S(1)}, u32[]{:S(2)}, u32[]{:S(2)}) async-start(bf16[16,80,128]{2,1,0:T(8,128)(2,1)} %get-tuple-element.12), calls=%async_computation.2 | async-start | bytes 655360 | tf_op jit(solution)/shard_map/all_to_all | solution.py:151

commit v3 on v2

--- a/solution.py
+++ b/solution.py
@@ -107,11 +107,20 @@
     squares_ref[...] = jnp.where(row == 0, key, value)
 
 
-def update_kernel(
+def update_kernel(*refs, rows, weight_rows, entries):
+    held, sems = refs[-11:-1], refs[-1]
+    inputs, outs = refs[:-21], refs[-21:-11]
+    copies = [pltpu.make_async_copy(held[i], outs[i], sems.at[i]) for i in range(len(outs))]
+    fill_outputs(*inputs, *held, copies=copies, rows=rows, weight_rows=weight_rows, entries=entries)
+    for copy in copies:
+        copy.wait()
+
+
+def fill_outputs(
     place_ref, data_ref, squares_ref, key_w, value_w, key_proj, value_proj, kf, ks, vf, vs,
     key_renewed, value_renewed, key_step, value_step,
     kf_new, ks_new, vf_new, vs_new, key_copy, value_copy,
-    *, rows, weight_rows, entries,
+    *, copies, rows, weight_rows, entries,
 ):
     own = pl.multiple_of(place_ref[0] * weight_rows, weight_rows)
     cores, chips = data_ref.shape[0], data_ref.shape[1]
@@ -125,6 +134,8 @@
         sn = SECOND_DECAY * second[...] + (1.0 - SECOND_DECAY) * projected * projected
         first_new[...] = fn
         second_new[...] = sn
+        copies[4 + 2 * which].start()
+        copies[5 + 2 * which].start()
         pair = jnp.concatenate(halves(fn / (jnp.sqrt(sn) + EPSILON)), axis=1)
         total = squares[which : which + 1]
         scale = LEARN_RATE * jnp.sqrt(total / entries)
@@ -137,6 +148,8 @@
         mine = steps_of(proj[pl.ds(own, weight_rows), :])
         step[...] = mine
         renewed[...] = w[...] - mine
+        copies[which].start()
+        copies[2 + which].start()
         everyone = steps_of(proj[...])
         at = rows + which * weight_rows
         for chip in range(chips):
@@ -144,6 +157,7 @@
                 r = ((chip + LEAD) % chips * cores + core) * weight_rows
                 old = data_ref[core, chip, at : at + weight_rows, :].astype(F32)
                 copy[r : r + weight_rows, :] = (old - everyone[r : r + weight_rows]).astype(BF16)
+        copies[8 + which].start()
 
 
 def swap(a, chips):
@@ -171,6 +185,7 @@
     sds = jax.ShapeDtypeStruct
     smem = pl.BlockSpec(memory_space=pltpu.SMEM)
     vmem = pl.BlockSpec(memory_space=pltpu.VMEM)
+    hbm = pl.BlockSpec(memory_space=pl.ANY)
 
     squares = pl.pallas_call(
         squares_kernel, out_shape=(sds((cores * lax.axis_size(TP[1]), 8, cols), F32),),
@@ -217,13 +232,16 @@
     moment = sds((rank, cols), F32)
     copy = sds((width, cols), BF16)
 
+    outs = (weight,) * 4 + (moment,) * 4 + (copy,) * 2
+
     def update(*refs):
         update_kernel(*refs, rows=rows, weight_rows=weight_rows, entries=entries)
 
     return pl.pallas_call(
         update,
-        out_shape=(weight,) * 4 + (moment,) * 4 + (copy,) * 2,
-        in_specs=[smem] + [vmem] * 10, out_specs=(vmem,) * 10, name="update",
+        out_shape=outs,
+        in_specs=[smem] + [vmem] * 10, out_specs=(hbm,) * 10, name="update",
+        scratch_shapes=[pltpu.VMEM(o.shape, o.dtype) for o in outs] + [pltpu.SemaphoreType.DMA((len(outs),))],
     )(
         place.reshape(1), data, near(squares), *map(near, (
             key_weight, value_weight, key_projector, value_projector,

time: 76.3 us -> 76.4 us (level)
  no operation moved by 1% of the time
where the time goes in v3:
time: 76.4 us; the launch traced here: 76 us
  blocking collectives  43.3 us (57%)
  starting transfers between devices  22.6 us (30%)
  Pallas kernels  8.26 us (11%)
  waiting for transfers between devices  1.16 us (2%)
    all_to_all x1, blocking collectives, swap(): return lax.all_to_all(a, Z, 0, 0)  18.7 us
    all_to_all x1, starting transfers between devices, body(): squares = lax.all_to_all(squares, (CORE, TP[1]), 0, 0)  17.4 us
    psum x1, blocking collectives, body(): squares = lax.psum(squares, TP[0])  14.2 us
    all_gather x1, blocking collectives, body(): data = near(lax.all_gather(message, CORE))  8.38 us
    all_to_all x1, starting transfers between devices, swap(): return lax.all_to_all(a, Z, 0, 0)  5.2 us
    pallas_call x1, Pallas kernels, body(): pl.pallas_call(project_kernel, out_shape=(pltpu.VMEM((2, rank, cols), BF1...  4.33 us
    all_gather x1, blocking collectives, body(): parts = near(lax.all_gather(parts, CORE))  1.99 us
    pallas_call x1, Pallas kernels, body(): pl.pallas_call(update, out_shape=outs, in_specs=[smem] + [vmem] * 10, out...  1.61 us
  transfers between devices with their start and end apart: 2, of which 1 were waited for; matrix products, arithmetic and copies ran while one was open for 0% of the time, Pallas kernels for 6%

profile of v3, /device:TPU:1, one launch (start us, length us, event | category | flops | bytes accessed | tf_op | source)
XLA Modules:
  0.0 76.0 jit_solution(10647238003788585080)
XLA Ops:
  0.6 0.0 copy-start.3
  0.7 0.0 copy-start.2
  0.7 1.5 %squares.1 = f32[8,8,128]{2,1,0:T(8,128)} custom-call(f32[32,128]{1,0:T(8,128)} %refs_3_.1, f32[32,128]{1,0:T(8,128)} %refs_4_.1), custom_call_target="tpu_custom_call" | custom-call | tf_op jit(solution)/shard_map/squares/pallas_call | solution.py:190
  2.2 17.4 %all-to-all-start = ((f32[8,8,128]{2,1,0:T(8,128)}), f32[8,8,128]{2,1,0:T(8,128)S(1)}, u32[]{:S(2)}, u32[]{:S(2)}) async-start(f32[8,8,128]{2,1,0:T(8,128)} %squares.1), calls=%async_computation | async-start | bytes 65536 | tf_op jit(solution)/shard_map/all_to_all | solution.py:194
  19.6 0.0 copy-start
  19.6 0.0 copy-start.1
  19.6 0.0 copy-start.4
  19.6 0.0 copy-start.5
  19.6 0.0 copy-start.6
  19.6 0.0 copy-start.7
  19.6 4.3 %project.1 = bf16[2,256,128]{2,1,0:T(8,128)(2,1)S(1)} custom-call(bf16[2048,1024]{1,0:T(8,128)(2,1)} %latent_hbm.1, bf16[2048,128]{1,0:T(8,128)(2,1)} %key_hbm.1, bf16[2048,128]{1,0:T(8,128)(2,1)} %value_hbm.1, bf16[1024,256]{1,0:T(8,128)(2,1)} %refs_5_.1, bf16[1024,256]{1,0:T(8,128)(2,1)} %refs_6_.1), custom_call_target="tpu_custom_call" | custom-call | tf_op jit(solution)/shard_map/project/pallas_call | solution.py:195
  23.9 2.0 %all-gather = bf16[4,256,128]{2,1,0:T(8,128)(2,1)S(1)} all-gather(bf16[2,256,128]{2,1,0:T(8,128)(2,1)S(1)} %project.1), channel_id=2, replica_groups=mesh['fs_0'=16,'fs_1'=2,'tp_0'=8,'tp_1'=4] {'fs_1'}, dimensions={0}, use_global_device_ids=true | all-gather | bytes 393216 | tf_op jit(solution)/shard_map/all_gather | solution.py:211
  25.9 0.0 all-to-all-done.squares_ref
  26.0 18.7 %all_to_all.15.pieces_ref = bf16[16,24,128]{2,1,0:T(8,128)(2,1)S(1)} all-to-all(bf16[16,24,128]{2,1,0:T(8,128)(2,1)S(1)} %cut.1), channel_id=1, replica_groups=mesh['fs_0'=16,'fs_1'=2,'tp_0'=8,'tp_1'=4] {'fs_0'}, dimensions={0} | all-to-all | bytes 196608 | tf_op jit(solution)/shard_map/all_to_all | solution.py:165
  44.7 0.0 copy-done.3
  44.7 0.0 copy-done.2
  44.7 0.8 spread.1
  45.5 5.2 %all-to-all-start.2 = ((bf16[16,80,128]{2,1,0:T(8,128)(2,1)}), bf16[16,80,128]{2,1,0:T(8,128)(2,1)S(1)}, u32[]{:S(2)}, u32[]{:S(2)}) async-start(bf16[16,80,128]{2,1,0:T(8,128)(2,1)} %get-tuple-element.12), calls=%async_computation.2 | async-start | bytes 655360 | tf_op jit(solution)/shard_map/all_to_all | solution.py:165
  50.7 14.2 %psum.7.refs_2_ = f32[8,128]{1,0:T(8,128)S(1)} all-reduce(f32[8,128]{1,0:T(8,128)S(1)} %get-tuple-element.13), channel_id=1, replica_groups=mesh['fs_0'=16,'fs_1'=2,'tp_0'=8,'tp_1'=4] {'tp_0'}, use_global_device_ids=true, to_apply=%region_0.0 | all-reduce | flops 1024 | bytes 8192 | tf_op jit(solution)/shard_map/psum | solution.py:227
  64.8 1.2 %all-to-all-done.2 = bf16[16,80,128]{2,1,0:T(8,128)(2,1)S(1)} async-done(((bf16[16,80,128]{2,1,0:T(8,128)(2,1)}), bf16[16,80,128]{2,1,0:T(8,128)(2,1)S(1)}, u32[]{:S(2)}, u32[]{:S(2)}) %all-to-all-start.2) | async-done | bytes 327712 | tf_op jit(solution)/shard_map/all_to_all | solution.py:165
  66.0 8.4 %all-gather.1 = bf16[32,80,128]{2,1,0:T(8,128)(2,1)S(1)} all-gather(bf16[16,80,128]{2,1,0:T(8,128)(2,1)S(1)} %all-to-all-done.2), channel_id=3, replica_groups=mesh['fs_0'=16,'fs_1'=2,'tp_0'=8,'tp_1'=4] {'fs_1'}, dimensions={0}, use_global_device_ids=true | all-gather | bytes 983040 | tf_op jit(solution)/shard_map/all_gather | solution.py:228
  74.4 0.0 copy-done
  74.4 0.0 copy-done.1
  74.4 0.0 copy-done.4
  74.4 0.0 copy-done.5
  74.4 0.0 copy-done.6
  74.4 0.0 copy-done.7
  74.4 1.6 %update.1 = (f32[32,128]{1,0:T(8,128)}, f32[32,128]{1,0:T(8,128)}, f32[32,128]{1,0:T(8,128)}, f32[32,128]{1,0:T(8,128)}, f32[256,128]{1,0:T(8,128)}, /*index=5*/...) custom-call(s32[1]{0:T(128)} %bitcast.refs_0_, ...), custom_call_target="tpu_custom_call" | custom-call | tf_op jit(solution)/shard_map/update/pallas_call | solution.py:240
  (1 shorter events, 0.0 us)
Async XLA Ops:
  0.6 44.1 %copy-start.3 = (f32[32,128]{1,0:T(8,128)S(1)}, f32[32,128]{1,0:T(8,128)}, u32[]{:S(2)}) copy-start(f32[32,128]{1,0:T(8,128)} %refs_4_.1) | copy-start | bytes 49156
  0.7 44.1 %copy-start.2 = (f32[32,128]{1,0:T(8,128)S(1)}, f32[32,128]{1,0:T(8,128)}, u32[]{:S(2)}) copy-start(f32[32,128]{1,0:T(8,128)} %refs_3_.1) | copy-start | bytes 49156
  2.2 23.8 %all-to-all-start = ((f32[8,8,128]{2,1,0:T(8,128)}), f32[8,8,128]{2,1,0:T(8,128)S(1)}, u32[]{:S(2)}, u32[]{:S(2)}) async-start(f32[8,8,128]{2,1,0:T(8,128)} %squares.1), calls=%async_computation | async-start | bytes 65536 | tf_op jit(solution)/shard_map/all_to_all | solution.py:194
  19.6 54.8 %copy-start = (bf16[1024,256]{1,0:T(8,128)(2,1)S(1)}, bf16[1024,256]{1,0:T(8,128)(2,1)}, u32[]{:S(2)}) copy-start(bf16[1024,256]{1,0:T(8,128)(2,1)} %refs_5_.1) | copy-start | bytes 1572868
  19.6 54.8 %copy-start.1 = (bf16[1024,256]{1,0:T(8,128)(2,1)S(1)}, bf16[1024,256]{1,0:T(8,128)(2,1)}, u32[]{:S(2)}) copy-start(bf16[1024,256]{1,0:T(8,128)(2,1)} %refs_6_.1) | copy-start | bytes 1572868
  19.6 54.8 %copy-start.4 = (f32[256,128]{1,0:T(8,128)S(1)}, f32[256,128]{1,0:T(8,128)}, u32[]{:S(2)}) copy-start(f32[256,128]{1,0:T(8,128)} %refs_7_.1) | copy-start | bytes 393220
  19.6 54.8 %copy-start.5 = (f32[256,128]{1,0:T(8,128)S(1)}, f32[256,128]{1,0:T(8,128)}, u32[]{:S(2)}) copy-start(f32[256,128]{1,0:T(8,128)} %refs_8_.1) | copy-start | bytes 393220
  19.6 54.8 %copy-start.6 = (f32[256,128]{1,0:T(8,128)S(1)}, f32[256,128]{1,0:T(8,128)}, u32[]{:S(2)}) copy-start(f32[256,128]{1,0:T(8,128)} %refs_9_.1) | copy-start | bytes 393220
  19.6 54.8 %copy-start.7 = (f32[256,128]{1,0:T(8,128)S(1)}, f32[256,128]{1,0:T(8,128)}, u32[]{:S(2)}) copy-start(f32[256,128]{1,0:T(8,128)} %refs_10_.1) | copy-start | bytes 393220
  45.5 20.5 %all-to-all-start.2 = ((bf16[16,80,128]{2,1,0:T(8,128)(2,1)}), bf16[16,80,128]{2,1,0:T(8,128)(2,1)S(1)}, u32[]{:S(2)}, u32[]{:S(2)}) async-start(bf16[16,80,128]{2,1,0:T(8,128)(2,1)} %get-tuple-element.12), calls=%async_computation.2 | async-start | bytes 655360 | tf_op jit(solution)/shard_map/all_to_all | solution.py:165
